TPU v7x, 128 devices: a whole 4x4x4 slice. The times are simulated.
128 devices in a mesh: sp: 16 (over z, y), tp: 8 (over x, core).
Axes of the slice: x: 4, y: 4, z: 4, core: 2. Of those that a mesh axis runs over, the one named last changes fastest.
Arguments:
- resid: bfloat16 [24576, 2048], P(('sp', 'tp')), may hold values from -6 to 6
- cond: bfloat16 [2048], P('sp'), may hold values from -6 to 6
- mod_shift: bfloat16 [2048, 2048], P('sp', 'tp'), may hold values from -0.125 to 0.125
- mod_scale: bfloat16 [2048, 2048], P('sp', 'tp'), may hold values from -0.125 to 0.125
- mod_gate: bfloat16 [2048, 2048], P('sp', 'tp'), may hold values from -0.125 to 0.125
- norm_gain: float32 [2048], replicated, may hold values from 0.1 to 1.9
- context: bfloat16 [1024, 2048], P('sp'), may hold values from -6 to 6
- w_query: bfloat16 [2048, 2048], P(None, 'tp'), may hold values from -0.125 to 0.125
- w_key: bfloat16 [2048, 2048], P(None, 'tp'), may hold values from -0.125 to 0.125
- w_value: bfloat16 [2048, 2048], P(None, 'tp'), may hold values from -0.125 to 0.125
- query_gain: float32 [128], replicated, may hold values from 0.5 to 6, as said below
- key_gain: float32 [128], replicated, may hold values from 0.5 to 6, as said below
- offset_bias: float32 [16, 15, 31], P('tp'), may hold values from -4 to 4
- context_bias: float32 [16], P('tp'), may hold values from -4.5 to 1
- w_out: bfloat16 [2048, 2048], replicated, may hold values from -0.5 to 0.5
Outputs:
- mixed: bfloat16 [24576, 2048], P(('sp', 'tp'))
Inputs may be any that keep to these rules, and one draw needn't show every extreme that they name: `query_gain`: positive gains. `key_gain`: positive gains.
All inputs are finite; a program needn't handle non-finite values.
Results may differ from a plain program's by a relative error of at most 0.0085.
The roundings to bfloat16 on the way count: a program that leaves them out, or rounds other values in their place, can miss the bound.
Values may be sent and summed in bfloat16 or wider, within the bound.
A program may use at most 128 MiB of HBM per device.

v0:
```python
import functools
import jax
import jax.numpy as jnp
from jax import lax
from jax.sharding import Mesh
from jax.sharding import PartitionSpec as P

HEAD_DIM = 128
GRID_W = 64
WIN_ROWS = 8
WIN_COLS = 16
R_DEV = 24
SP = ("sp_0", "sp_1")
SP_TP = ("sp_0", "sp_1", "tp")
EPS = 1e-06


def over_axes(shard, axes):
    return functools.reduce(lax.psum, axes, shard)


def gather_turned(arrays, axis, dims):
    turned = [jnp.moveaxis(a, dim, 0) for a, dim in zip(arrays, dims)]
    widths = [t[0].size for t in turned]
    both = jnp.concatenate([t.reshape(-1, w) for t, w in zip(turned, widths)], axis=1)
    filled = lax.all_gather(both, axis, axis=0, tiled=True)
    blocks = jnp.split(filled, [sum(widths[:k]) for k in range(1, len(widths))], axis=1)
    return tuple(
        (
            jnp.moveaxis(b.reshape(-1, *t.shape[1:]), 0, dim)
            for b, t, dim in zip(blocks, turned, dims)
        )
    )


def side_by_side(arrays, axis, dim, along):
    both = jnp.concatenate(arrays, axis=along)
    filled, at, done = (lax.all_gather(both, axis, axis=dim, tiled=True), 0, [])
    for a in arrays:
        done.append(lax.slice_in_dim(filled, at, at + a.shape[along], axis=along))
        at += a.shape[along]
    return tuple(done)


def padded_2(cells, sides, width):
    for axis, dim in sides:
        count = lax.axis_size(axis)
        ends = count - 1
        head = lax.slice_in_dim(cells, 0, width, axis=dim)
        tail = lax.slice_in_dim(cells, cells.shape[dim] - width, cells.shape[dim], axis=dim)
        cells = jnp.concatenate(
            [
                lax.ppermute(tail, axis, [(i, (i + 1) % count) for i in range(ends)]),
                cells,
                lax.ppermute(head, axis, [((i + 1) % count, i) for i in range(ends)]),
            ],
            axis=dim,
        )
    return cells


def head_norm(values, gain, heads_local):
    count = values.shape[0]
    split = values.reshape(count, heads_local, -1)
    scaled = split * lax.rsqrt(jnp.mean(split * split, axis=-1, keepdims=True) + EPS) * gain
    return scaled.reshape(count, -1).astype(jnp.bfloat16)


def project_context(rows_in, norm_gain, w_key, w_value, key_gain, heads_local):
    floats = rows_in.astype(jnp.float32)
    inverse = lax.rsqrt(jnp.mean(floats * floats, axis=-1, keepdims=True) + EPS)
    normed = (floats * inverse * norm_gain).astype(jnp.bfloat16)
    keys = head_norm(
        jnp.dot(normed, w_key, preferred_element_type=jnp.float32), key_gain, heads_local
    )
    values = jnp.dot(normed, w_value, preferred_element_type=jnp.float32).astype(jnp.bfloat16)
    return (keys, values)


def attend_rows(
    queries, key_at, value_at, row_offset, offset_bias, ctx_key, ctx_value, context_bias
):
    grid_w = queries.shape[1]
    columns = jnp.arange(grid_w, dtype=jnp.int32)
    col_begin = jnp.clip(columns - WIN_COLS // 2, 0, grid_w - WIN_COLS)
    valid = (columns[None, :] >= col_begin[:, None]) & (
        columns[None, :] < col_begin[:, None] + WIN_COLS
    )
    col_offset = jnp.clip(columns[None, :] - columns[:, None] + WIN_COLS - 1, 0, 2 * WIN_COLS - 2)
    col_onehot = (col_offset[..., None] == jnp.arange(2 * WIN_COLS - 1, dtype=jnp.int32)).astype(
        jnp.float32
    )
    row_onehot = (
        row_offset[:, :, None] == jnp.arange(2 * WIN_ROWS - 1, dtype=jnp.int32)[None, None, :]
    ).astype(jnp.float32)
    bias = jnp.einsum(
        "nir,hrj,ckj->nhcik", row_onehot, offset_bias, col_onehot, precision=lax.Precision.HIGHEST
    )
    factor = HEAD_DIM ** (-0.5)
    s_win = (
        jnp.stack(
            [
                jnp.einsum(
                    "nchd,nkhd->nhck", queries, key_at(i), preferred_element_type=jnp.float32
                )
                for i in range(WIN_ROWS)
            ],
            axis=3,
        )
        * factor
        + bias
    )
    s_win = jnp.where(valid[None, None, :, None, :], s_win, -1e30)
    s_ctx = (
        jnp.einsum("nchd,jhd->nhcj", queries, ctx_key, preferred_element_type=jnp.float32) * factor
    )
    s_ctx = s_ctx + context_bias[None, :, None, None]
    top = jnp.maximum(jnp.max(s_win, axis=(3, 4)), jnp.max(s_ctx, axis=3))
    e_win = jnp.exp(s_win - top[..., None, None])
    e_ctx = jnp.exp(s_ctx - top[..., None])
    total = jnp.sum(e_win, axis=(3, 4)) + jnp.sum(e_ctx, axis=3)
    p_win = (e_win / total[..., None, None]).astype(jnp.bfloat16)
    p_ctx = (e_ctx / total[..., None]).astype(jnp.bfloat16)
    out = jnp.einsum("nhcj,jhd->nchd", p_ctx, ctx_value, preferred_element_type=jnp.float32)
    for i in range(WIN_ROWS):
        out = out + jnp.einsum(
            "nhck,nkhd->nchd", p_win[:, :, :, i], value_at(i), preferred_element_type=jnp.float32
        )
    count = queries.shape[0]
    return out.astype(jnp.bfloat16).reshape(count * grid_w, -1)


def shards(
    resid,
    cond,
    mod_shift,
    mod_scale,
    mod_gate,
    norm_gain,
    context,
    w_query,
    w_key,
    w_value,
    query_gain,
    key_gain,
    offset_bias,
    context_bias,
    w_out,
):
    heads_local = offset_bias.shape[0]
    width = w_query.shape[1]
    lifted = jax.nn.silu(cond.astype(jnp.float32)).astype(jnp.bfloat16)
    shift_part = jnp.dot(lifted, mod_shift, preferred_element_type=jnp.float32)
    scale_part = jnp.dot(lifted, mod_scale, preferred_element_type=jnp.float32)
    gate_part = jnp.dot(lifted, mod_gate, preferred_element_type=jnp.float32)
    summed = (over_axes(shift_part, SP), over_axes(scale_part, SP), over_axes(gate_part, SP))
    shift, scale, gate = gather_turned((summed[0], summed[1], summed[2]), "tp", (0, 0, 0))
    floats = resid.astype(jnp.float32)
    inverse = lax.rsqrt(jnp.mean(floats * floats, axis=-1, keepdims=True) + EPS)
    normed = (floats * inverse * norm_gain * (1.0 + scale) + shift).astype(jnp.bfloat16)
    piece = lax.all_gather(normed, "tp", axis=0, tiled=True)
    queries = head_norm(
        jnp.dot(piece, w_query, preferred_element_type=jnp.float32), query_gain, heads_local
    )
    keys = head_norm(
        jnp.dot(piece, w_key, preferred_element_type=jnp.float32), key_gain, heads_local
    )
    values = jnp.dot(piece, w_value, preferred_element_type=jnp.float32).astype(jnp.bfloat16)
    projected = jnp.concatenate([queries, keys, values], axis=1)
    query = projected[:, :width]
    key_value = projected[:, width:]
    own_key, own_value = project_context(context, norm_gain, w_key, w_value, key_gain, heads_local)
    ctx_key, ctx_value = side_by_side((own_key, own_value), SP, 0, 1)
    ctx_count = ctx_key.shape[0]
    ctx_key = ctx_key.reshape(ctx_count, heads_local, HEAD_DIM)
    ctx_value = ctx_value.reshape(ctx_count, heads_local, HEAD_DIM)
    reach = WIN_ROWS // 2
    grid = key_value.reshape(R_DEV, GRID_W, 2 * width)
    padded = padded_2(grid, ((SP, 0),), reach)
    padded = padded.reshape(R_DEV + 2 * reach, GRID_W, 2, heads_local, HEAD_DIM)
    total_rows = R_DEV * lax.axis_size(SP)
    first = lax.axis_index(SP) * R_DEV
    global_rows = first + jnp.arange(R_DEV, dtype=jnp.int32)
    row_start = jnp.clip(global_rows - reach, 0, total_rows - WIN_ROWS)
    window_rows = jnp.arange(WIN_ROWS, dtype=jnp.int32)[None, :]
    row_offset = row_start[:, None] + window_rows - global_rows[:, None] + WIN_ROWS - 1
    queries = query.reshape(R_DEV, GRID_W, heads_local, HEAD_DIM)
    upper = min(reach, R_DEV)
    lower = max(upper, R_DEV - reach)
    edge_rows = list(range(upper)) + list(range(lower, R_DEV))
    edge_index = jnp.array(edge_rows, dtype=jnp.int32)
    edge_window = (jnp.take(row_start, edge_index) - first + reach)[:, None] + window_rows
    edge_kv = jnp.take(padded, edge_window, axis=0)
    edge_out = attend_rows(
        jnp.take(queries, edge_index, axis=0),
        lambda i: edge_kv[:, i, :, 0],
        lambda i: edge_kv[:, i, :, 1],
        jnp.take(row_offset, edge_index, axis=0),
        offset_bias,
        ctx_key,
        ctx_value,
        context_bias,
    )
    pieces = [edge_out[: upper * GRID_W]]
    middle = lower - upper
    inner_out = attend_rows(
        queries[upper:lower],
        lambda i: padded[upper + i : upper + i + middle, :, 0],
        lambda i: padded[upper + i : upper + i + middle, :, 1],
        row_offset[upper:lower],
        offset_bias,
        ctx_key,
        ctx_value,
        context_bias,
    )
    pieces.append(inner_out)
    pieces.append(edge_out[upper * GRID_W :])
    attended = jnp.concatenate(pieces, axis=0)
    full_rows = lax.all_to_all(attended, "tp", split_axis=0, concat_axis=1, tiled=True)
    result = jnp.dot(full_rows, w_out, preferred_element_type=jnp.float32)
    return (floats + gate * result).astype(jnp.bfloat16)


def solution(mesh):
    split = Mesh(mesh.devices.reshape(4, 4, mesh.shape["tp"]), ("sp_0", "sp_1", "tp"))
    placed = (
        P(SP_TP, None),
        P(SP),
        P(SP, "tp"),
        P(SP, "tp"),
        P(SP, "tp"),
        P(),
        P(SP, None),
        P(None, "tp"),
        P(None, "tp"),
        P(None, "tp"),
        P(),
        P(),
        P("tp", None, None),
        P("tp"),
        P(),
    )
    return jax.shard_map(
        shards, mesh=split, in_specs=placed, out_specs=P(SP_TP, None), check_vma=False
    )
```

profile of v0, /device:TPU:24, one launch (start us, length us, event | category | flops | bytes accessed | tf_op | source)
XLA Modules:
  0.0 245.6 jit_solution(12134459745243298402)
XLA Ops:
  6.6 0.8 broadcast_bitcast_fusion.1
  7.4 1.1 fusion.59
  8.5 1.3 fusion.143
  10.0 1.7 convolution_convert_fusion.1
  12.5 1.0 fusion.128
  13.5 1.0 fusion.126
  14.5 1.0 fusion.124
  15.5 11.7 %all-reduce.1 = (f32[256]{0:T(256)S(1)}, f32[256]{0:T(256)S(1)}, f32[256]{0:T(256)S(1)}) all-reduce(f32[256]{0:T(256)S(1)} %bitcast.451, f32[256]{0:T(256)S(1)} %bitcast.450, f32[256]{0:T(256)S(1)} %bitcast.449), channel_id=1, replica_groups=mesh['sp_0'=4,'sp_1'=4,'tp'=8] {'sp_0'}, use_global_device_ids=true, to_apply=%region_4.5 | all-reduce | flops 768 | bytes 6144 | tf_op jit(solution)/shard_map/psum | solution.py:19
  27.3 7.5 %all-reduce = (f32[256,1]{0,1:T(1,128)S(1)}, f32[256,1]{0,1:T(1,128)S(1)}, f32[256,1]{0,1:T(1,128)S(1)}) all-reduce(f32[256,1]{0,1:T(1,128)S(1)} %bitcast.452, f32[256,1]{0,1:T(1,128)S(1)} %bitcast.453, f32[256,1]{0,1:T(1,128)S(1)} %bitcast.454), channel_id=1, replica_groups=mesh['sp_0'=4,'sp_1'=4,'tp'=8] {'sp_1'}, use_global_device_ids=true, to_apply=%region_5.6 | all-reduce | flops 768 | bytes 6144 | tf_op jit(solution)/shard_map/psum | solution.py:19
  34.7 13.3 %all_gather.9 = f32[2048,3]{0,1:T(4,128)S(1)} all-gather(f32[256,3]{0,1:T(4,128)S(1)} %pad_maximum_fusion.4), channel_id=1, replica_groups=mesh['sp_0'=4,'sp_1'=4,'tp'=8] {'tp'}, dimensions={0}, use_global_device_ids=true | all-gather | bytes 27648 | tf_op jit(solution)/shard_map/all_gather | solution.py:26
  48.3 1.2 fusion.16
  51.6 6.1 %fusion.111 = f32[64,64,2,16,8]{1,3,4,2,0:T(8,128)} fusion(f32[64,64,2,15,1]{1,3,4,2,0:T(8,128)S(1)} %convolution_bitcast_fusion.16, s32[16,8]{0,1:T(8,128)S(1)} %copy.538), kind=kOutput, calls=%fused_computation.234 | convolution fusion | flops 188745600 | bytes 4686336 | tf_op jit(solution)/shard_map/nir,hrj,ckj->nhcik/dot_general | solution.py:96
  57.7 9.6 %copy.539 = f32[64,64,2,16,8]{0,1,2,3,4:T(8,128)} copy(f32[64,64,2,16,8]{1,3,4,2,0:T(8,128)} %fusion.111) | data formatting | bytes 8388608 | tf_op jit(solution)/shard_map/nir,hrj,ckj->nhcik/dot_general | solution.py:96
  67.5 3.8 %fusion.116 = f32[64,64,2,8,8]{1,4,3,2,0:T(8,128)} fusion(f32[64,64,2,15,1]{1,3,4,2,0:T(8,128)S(1)} %convolution_bitcast_fusion.16, s32[8,8]{1,0:T(8,128)S(1)} %gather_fusion.3), kind=kOutput, calls=%fused_computation.243 | convolution fusion | flops 94372800 | bytes 2588928 | tf_op jit(solution)/shard_map/nir,hrj,ckj->nhcik/dot_general | solution.py:96
  71.3 5.6 %copy.496 = f32[64,64,2,8,8]{0,1,2,3,4:T(8,128)} copy(f32[64,64,2,8,8]{1,4,3,2,0:T(8,128)} %fusion.116) | data formatting | bytes 4194304 | tf_op jit(solution)/shard_map/nir,hrj,ckj->nhcik/dot_general | solution.py:96
  77.0 2.2 fusion.140
  79.2 0.9 reshape.300
  80.1 19.1 %all-gather.5.cloned.1.call-done = bf16[1536,2048]{1,0:T(8,128)(2,1)} async-done(((bf16[192,2048]{1,0:T(8,128)(2,1)}), bf16[1536,2048]{1,0:T(8,128)(2,1)}) %all-gather.5.cloned.1.call-update) | async-done | bytes 6291472 | tf_op jit(solution)/shard_map/all_gather | solution.py:161
  99.2 4.8 %bitcast_reduce_fusion.2 = (f32[1536,2]{0,1:T(2,128)S(1)}, f32[1536,256]{0,1:T(8,128)S(1)}) fusion(bf16[1536,2048]{1,0:T(8,128)(2,1)} %all-gather.5.cloned.1.call-done, bf16[2048,256]{1,0:T(8,128)(2,1)S(1)} %copy-done), kind=kOutput, calls=%fused_computation.49 | convolution fusion | flops 1611396096 | bytes 8925184 | tf_op jit(solution)/shard_map/dot_general | solution.py:166
  104.3 1.9 convolution_convert_fusion
  106.3 1.6 copy.489
  107.9 2.4 concatenate.26
  110.3 8.0 %fusion.139 = (bf16[16,64,1,2,128]{4,3,2,1,0:T(2,128)(2,1)}, bf16[16,64,1,2,128]{4,3,2,1,0:T(2,128)(2,1)}, bf16[16,64,1,2,128]{4,3,2,1,0:T(2,128)(2,1)}, bf16[16...) fusion(bf16[24,64,2,2,128]{4,3,2,1,0:T(2,128)(2,1)S(1)} %concat, ...), kind=kLoop, calls=%fused_computation.286 | loop fusion | bytes 16777216 | tf_op jit(solution)/shard_map/slice | solution.py:209
  118.3 4.7 %bitcast_reduce_fusion.3 = (f32[1536,2]{0,1:T(2,128)S(1)}, f32[1536,256]{0,1:T(8,128)S(1)}) fusion(bf16[1536,2048]{1,0:T(8,128)(2,1)} %all-gather.5.cloned.1.call-done, bf16[2048,256]{1,0:T(8,128)(2,1)S(1)} %copy-done.41), kind=kOutput, calls=%fused_computation.53 | convolution fusion | flops 1611396096 | bytes 8925184 | tf_op jit(solution)/shard_map/dot_general | solution.py:163
  123.2 0.9 slice.299
  124.2 2.0 copy.519
  126.3 1.2 slice.232
  127.6 1.5 fusion.37
  129.1 1.5 fusion.36
  133.1 3.3 %copy-done.7 = f32[16,2,64,8,64]{2,4,1,0,3:T(8,128)} copy-done((f32[16,2,64,8,64]{2,4,1,0,3:T(8,128)}, f32[16,2,64,8,64]{2,4,1,0,3:T(8,128)S(1)}, u32[]{:S(2)}) %copy-start.7) | copy-done | bytes 4194328
  136.4 1.3 fusion.62
  137.7 3.2 %copy-done.2 = f32[2,1024,1024]{1,2,0} copy-done((f32[2,1024,1024]{1,2,0}, f32[2,1024,1024]{1,2,0:S(1)}, u32[]{:S(2)}) %copy-start.2) | copy-done | bytes 8388632
  140.9 0.9 bitcast_reduce_fusion
  141.8 12.2 %fusion.135 = (f32[16,2,64]{2,1,0:T(2,128)S(1)}, f32[16,2,64,8,64]{2,4,1,0,3:T(8,128)}) fusion(f32[64,64,2,16,8]{0,1,2,3,4:T(8,128)} %copy.539, f32[16,2,64,8,64]{2,4,1,0,3:T(8,128)} %copy-done.7, pred[64,64]{0,1:T(8,128)(4,1)S(1)} %fusion.114), kind=kLoop, calls=%fused_computation.284 | loop fusion | flops 4192256 | bytes 12595200 | tf_op jit(solution)/shard_map/reduce_max | solution.py:118
  154.1 4.5 %fusion.3 = f32[16,2,64]{2,0,1:T(8,128)S(1)} fusion(f32[2,1024,16,64]{1,3,2,0:T(8,128)} %bitcast.426, f32[16,2,64]{2,0,1:T(8,128)S(1)} %copy_maximum_fusion, f32[2]{0:T(128)S(1)} %copy-done.38), kind=kLoop, calls=%fused_computation.14 | loop fusion | flops 8386560 | bytes 8405000 | tf_op jit(solution)/shard_map/reduce_sum | solution.py:121
  158.6 1.6 copy.492
  160.2 0.9 fusion.79
  161.1 1.1 reshape.354
  162.3 4.8 %fusion.2 = f32[16,2,64]{2,1,0:T(2,128)S(1)} fusion(f32[16,2,64,8,64]{2,4,1,0,3:T(8,128)} %get-tuple-element.12, f32[16,2,64]{2,1,0:T(2,128)S(1)} %copy.541), kind=kLoop, calls=%fused_computation.13 | loop fusion | flops 2095104 | bytes 4210688 | tf_op jit(solution)/shard_map/reduce_sum | solution.py:121
  167.1 4.3 %divide_convert_fusion = bf16[16,2,64,8,64]{2,4,1,0,3:T(8,128)(2,1)S(1)} fusion(f32[16,2,64,8,64]{2,4,1,0,3:T(8,128)} %get-tuple-element.12, f32[16,2,64]{2,1,0:T(2,128)S(1)} %copy.545, f32[16,2,64]{2,1,0:T(2,128)S(1)} %copy.541), kind=kLoop, calls=%fused_computation.9 | loop fusion | flops 3145728 | bytes 6307840 | tf_op jit(solution)/shard_map/convert_element_type | solution.py:122
  171.4 1.8 slice_bitcast_fusion
  173.2 1.5 copy-done.3
  174.8 2.2 fusion.21
  180.8 0.9 copy.752
  181.7 0.8 copy.488
  182.5 3.4 %collective-permute-start = (bf16[4,64,512]{2,1,0:T(8,128)(2,1)}, bf16[4,64,512]{2,1,0:T(8,128)(2,1)}, u32[]{:S(2)}, u32[]{:S(2)}) collective-permute-start(bf16[4,64,512]{2,1,0:T(8,128)(2,1)} %bitcast.23), channel_id=1, source_target_pairs={{0,8},{8,16},{16,24},{24,32},{32,40},{40,48},{48,56},{56,64},{64,7... | collective-permute-start | bytes 786440 | tf_op jit(solution)/shard_map/ppermute | solution.py:53
  185.9 0.9 copy.490
  186.8 2.4 collective-permute-start.1
  189.2 1.2 copy.485
  191.1 0.7 fusion.64
  191.8 1.9 copy-done.4
  194.3 1.0 concatenate.25
  195.4 3.9 %collective-permute-done.1 = bf16[4,64,512]{2,1,0:T(8,128)(2,1)} collective-permute-done((bf16[4,64,512]{2,1,0:T(8,128)(2,1)}, bf16[4,64,512]{2,1,0:T(8,128)(2,1)}, u32[]{:S(2)}, u32[]{:S(2)}) %collective-permute-start.1) | collective-permute-done | bytes 262176 | tf_op jit(solution)/shard_map/ppermute | solution.py:55
  199.3 1.0 concatenate.27
  200.3 1.7 pad_maximum_fusion
  202.0 3.1 %gather_fusion.2 = bf16[64,64,2,2,128]{4,1,3,2,0:T(8,128)(2,1)} fusion(bf16[32,64,2,2,128]{4,1,3,2,0:T(8,128)(2,1)S(1)} %pad_maximum_fusion, s32[1024]{0:T(1024)S(1)} %pad_clamp_fusion), kind=kCustom, calls=%fused_computation.2 | custom fusion | bytes 8388864 | tf_op jit(solution)/shard_map/jit(_take)/gather | solution.py:193
  205.1 2.6 %copy_select_fusion = bf16[8,8,64,2,2,128]{5,2,4,0,3,1:T(8,128)(2,1)S(1)} fusion(bf16[8,8,64,2,2,128]{5,2,4,3,1,0:T(8,128)(2,1)} %bitcast.431, pred[8,8]{0,1:T(8,128)(4,1)S(1)} %fusion.123), kind=kLoop, calls=%fused_computation.20 | loop fusion | flops 2097152 | bytes 8388672 | tf_op jit(solution)/shard_map/jit(_take)/select_n | solution.py:193
  210.0 1.6 fusion.137
  212.2 1.0 fusion.8
  213.2 0.7 fusion.7
  213.9 1.3 fusion.39
  215.6 0.7 divide_convert_fusion.2
  219.5 16.2 %all_to_all.19 = bf16[8,192,256]{2,1,0:T(8,128)(2,1)S(1)} all-to-all(bf16[8,192,256]{2,1,0:T(8,128)(2,1)S(1)} %bitcast.432), channel_id=1, replica_groups=mesh['sp_0'=4,'sp_1'=4,'tp'=8] {'tp'}, dimensions={0} | all-to-all | bytes 1572864 | tf_op jit(solution)/shard_map/all_to_all | solution.py:219
  235.8 2.7 %fusion.10 = bf16[192,2048]{1,0:T(8,128)(2,1)} fusion(bf16[192,2048]{1,0:T(8,128)(2,1)S(1)} %bitcast.438, bf16[2048,2048]{1,0:T(8,128)(2,1)S(1)} %bitcast.456, bf16[192,2048]{1,0:T(8,128)(2,1)S(1)} %copy-done.13, f32[2048]{0:T(1024)S(1)} %bitcast.448), kind=kOutput, calls=%fused_computation.31 | convolution fusion | flops 1612185600 | bytes 10756096 | tf_op jit(solution)/shard_map/dot_general | solution.py:220
  (180 shorter events, 17.9 us)
Async XLA Ops:
  6.5 2.0 copy-start
  6.5 43.1 %copy-start.39 = (s32[8]{0:T(128)S(1)}, s32[8]{0:T(128)}, u32[]{:S(2)}) copy-start(s32[8]{0:T(128)} %constant.138) | copy-start | bytes 100
  6.5 41.7 %copy-start.36 = (f32[2048]{0:T(1024)S(1)}, f32[2048]{0:T(1024)}, u32[]{:S(2)}) copy-start(f32[2048]{0:T(1024)} %param.21) | copy-start | bytes 24580
  6.5 41.5 %copy-start.12 = (bf16[192,2048]{1,0:T(8,128)(2,1)S(1)}, bf16[192,2048]{1,0:T(8,128)(2,1)}, u32[]{:S(2)}) copy-start(bf16[192,2048]{1,0:T(8,128)(2,1)} %param.16) | copy-start | bytes 2359300
  6.5 44.4 %copy-start.37 = (f32[2,15,31]{2,0,1:T(2,128)S(1)}, f32[2,15,31]{2,0,1:T(2,128)}, u32[]{:S(2)}) copy-start(f32[2,15,31]{2,0,1:T(2,128)} %param.28) | copy-start | bytes 11164
  6.5 70.4 %all-gather.3.cloned.1.call-start = ((), (), s32[]{:S(2)}) async-start(), calls=%async_computation.1 | async-start | bytes 1114112 | tf_op jit(solution)/shard_map/all_gather | solution.py:38
  12.5 86.7 %all-gather.5.cloned.1.call-start = ((), (), s32[]{:S(2)}) async-start(), calls=%async_computation.2 | async-start | bytes 7077888 | tf_op jit(solution)/shard_map/all_gather | solution.py:161
  71.3 5.6 %copy-start.42 = (f32[128]{0:T(128)S(1)}, f32[128]{0:T(128)}, u32[]{:S(2)}) copy-start(f32[128]{0:T(128)} %param.26) | copy-start | bytes 1540
  80.1 24.1 %copy-start.31 = (bf16[2048,256]{1,0:T(8,128)(2,1)S(1)}, bf16[2048,256]{1,0:T(8,128)(2,1)}, u32[]{:S(2)}) copy-start(bf16[2048,256]{1,0:T(8,128)(2,1)} %param.25) | copy-start | bytes 3145732
  99.2 5.0 %copy-start.40 = (bf16[1536,2048]{1,0:T(8,128)(2,1)S(1)}, bf16[1536,2048]{1,0:T(8,128)(2,1)}, u32[]{:S(2)}) copy-start(bf16[1536,2048]{1,0:T(8,128)(2,1)} %all-gather.5.cloned.1.call-done) | copy-start | bytes 18874372
  106.2 4.1 %copy-start.14 = (bf16[1536,256]{0,1:T(8,128)(2,1)}, bf16[1536,256]{0,1:T(8,128)(2,1)S(1)}, u32[]{:S(2)}) copy-start(bf16[1536,256]{0,1:T(8,128)(2,1)S(1)} %convolution_convert_fusion) | copy-start | bytes 2359300
  110.2 8.0 %copy-start.41 = (bf16[2048,256]{1,0:T(8,128)(2,1)S(1)}, bf16[2048,256]{1,0:T(8,128)(2,1)}, u32[]{:S(2)}) copy-start(bf16[2048,256]{1,0:T(8,128)(2,1)} %param.23) | copy-start | bytes 3145732
  123.2 1.1 copy-start.8
  126.3 4.8 %copy-start.29 = (bf16[16,64,1,2,128]{4,3,2,1,0:T(2,128)(2,1)S(1)}, bf16[16,64,1,2,128]{4,3,2,1,0:T(2,128)(2,1)}, u32[]{:S(2)}) copy-start(bf16[16,64,1,2,128]{4,3,2,1,0:T(2,128)(2,1)} %get-tuple-element.50) | copy-start | bytes 1572868
  127.5 3.1 %copy-start.30 = (bf16[16,64,1,2,128]{4,3,2,1,0:T(2,128)(2,1)S(1)}, bf16[16,64,1,2,128]{4,3,2,1,0:T(2,128)(2,1)}, u32[]{:S(2)}) copy-start(bf16[16,64,1,2,128]{4,3,2,1,0:T(2,128)(2,1)} %get-tuple-element.51) | copy-start | bytes 1572868
  127.6 3.8 %copy-start.28 = (bf16[16,64,1,2,128]{4,3,2,1,0:T(2,128)(2,1)S(1)}, bf16[16,64,1,2,128]{4,3,2,1,0:T(2,128)(2,1)}, u32[]{:S(2)}) copy-start(bf16[16,64,1,2,128]{4,3,2,1,0:T(2,128)(2,1)} %get-tuple-element.49) | copy-start | bytes 1572868
  129.1 2.8 %copy-start.27 = (bf16[16,64,1,2,128]{4,3,2,1,0:T(2,128)(2,1)S(1)}, bf16[16,64,1,2,128]{4,3,2,1,0:T(2,128)(2,1)}, u32[]{:S(2)}) copy-start(bf16[16,64,1,2,128]{4,3,2,1,0:T(2,128)(2,1)} %get-tuple-element.48) | copy-start | bytes 1572868
  130.6 1.6 copy-start.26
  131.1 1.6 copy-start.25
  131.5 4.9 %copy-start.10 = (bf16[128,2,8,128]{3,2,1,0:T(8,128)(2,1)S(1)}, bf16[128,2,8,128]{3,2,1,0:T(8,128)(2,1)}, u32[]{:S(2)}) copy-start(bf16[128,2,8,128]{3,2,1,0:T(8,128)(2,1)} %get-tuple-element.58) | copy-start | bytes 1572868
  133.1 3.3 %copy-start.7 = (f32[16,2,64,8,64]{2,4,1,0,3:T(8,128)}, f32[16,2,64,8,64]{2,4,1,0,3:T(8,128)S(1)}, u32[]{:S(2)}) copy-start(f32[16,2,64,8,64]{2,4,1,0,3:T(8,128)S(1)} %fusion.30) | copy-start | bytes 12582916
  136.4 4.5 %copy-start.38 = (f32[2]{0:T(128)S(1)}, f32[2]{0:T(128)}, u32[]{:S(2)}) copy-start(f32[2]{0:T(128)} %param.29) | copy-start | bytes 28
  137.6 3.2 %copy-start.2 = (f32[2,1024,1024]{1,2,0}, f32[2,1024,1024]{1,2,0:S(1)}, u32[]{:S(2)}) copy-start(f32[2,1024,1024]{1,2,0:S(1)} %fusion.62) | copy-start | bytes 25165828
  154.1 6.2 %copy-start.15 = (bf16[1536,256]{0,1:T(8,128)(2,1)S(1)}, bf16[1536,256]{0,1:T(8,128)(2,1)}, u32[]{:S(2)}) copy-start(bf16[1536,256]{0,1:T(8,128)(2,1)} %copy-done.14) | copy-start | bytes 2359300
  158.6 2.5 %copy-start.9 = (bf16[1536,256]{0,1:T(8,128)(2,1)S(1)}, bf16[1536,256]{0,1:T(8,128)(2,1)}, u32[]{:S(2)}) copy-start(bf16[1536,256]{0,1:T(8,128)(2,1)} %copy-done.8) | copy-start | bytes 2359300
  167.1 6.2 %copy-start.34 = (bf16[1024,2,128]{2,1,0:T(2,128)(2,1)S(1)}, bf16[1024,2,128]{2,1,0:T(2,128)(2,1)}, u32[]{:S(2)}) copy-start(bf16[1024,2,128]{2,1,0:T(2,128)(2,1)} %reshape.300) | copy-start | bytes 1572868
  171.4 3.4 %copy-start.3 = (f32[2,1024,1024]{1,2,0:S(1)}, f32[2,1024,1024]{1,2,0}, u32[]{:S(2)}) copy-start(f32[2,1024,1024]{1,2,0} %copy-done.2) | copy-start | bytes 25165828
  174.8 2.2 copy-start.24
  174.8 2.6 %copy-start.23 = (bf16[16,64,1,2,128]{4,3,2,1,0:T(2,128)(2,1)S(1)}, bf16[16,64,1,2,128]{4,3,2,1,0:T(2,128)(2,1)}, u32[]{:S(2)}) copy-start(bf16[16,64,1,2,128]{4,3,2,1,0:T(2,128)(2,1)} %get-tuple-element.44) | copy-start | bytes 1572868
  176.9 1.0 copy-start.22
  177.0 1.4 copy-start.21
  177.3 1.4 copy-start.20
  178.0 1.1 copy-start.19
  178.4 1.1 copy-start.18
  178.7 1.1 copy-start.16
  179.5 2.2 copy-start.33
  179.5 6.4 %copy-start.32 = (bf16[256,512]{0,1:T(8,128)(2,1)S(1)}, bf16[256,512]{0,1:T(8,128)(2,1)}, u32[]{:S(2)}) copy-start(bf16[256,512]{0,1:T(8,128)(2,1)} %get-tuple-element.56) | copy-start | bytes 786436
  179.9 11.2 %copy-start.11 = (bf16[128,2,8,128]{3,2,1,0:T(8,128)(2,1)S(1)}, bf16[128,2,8,128]{3,2,1,0:T(8,128)(2,1)}, u32[]{:S(2)}) copy-start(bf16[128,2,8,128]{3,2,1,0:T(8,128)(2,1)} %get-tuple-element.58) | copy-start | bytes 1572868
  182.5 11.8 %collective-permute-start = (bf16[4,64,512]{2,1,0:T(8,128)(2,1)}, bf16[4,64,512]{2,1,0:T(8,128)(2,1)}, u32[]{:S(2)}, u32[]{:S(2)}) collective-permute-start(bf16[4,64,512]{2,1,0:T(8,128)(2,1)} %bitcast.23), channel_id=1, source_target_pairs={{0,8},{8,16},{16,24},{24,32},{32,40},{40,48},{48,56},{56,64},{64,7... | collective-permute-start | bytes 786440 | tf_op jit(solution)/shard_map/ppermute | solution.py:53
  186.8 12.5 %collective-permute-start.1 = (bf16[4,64,512]{2,1,0:T(8,128)(2,1)}, bf16[4,64,512]{2,1,0:T(8,128)(2,1)}, u32[]{:S(2)}, u32[]{:S(2)}) collective-permute-start(bf16[4,64,512]{2,1,0:T(8,128)(2,1)} %bitcast.24), channel_id=1, source_target_pairs={{8,0},{16,8},{24,16},{32,24},{40,32},{48,40},{56,48},{64,56},{72,6... | collective-permute-start | bytes 786440 | tf_op jit(solution)/shard_map/ppermute | solution.py:55
  191.8 2.0 copy-start.4
  207.7 2.2 copy-start.6
  210.0 2.2 copy-start.5
  212.2 1.8 copy-start.35
  216.3 19.4 %slice-start = ((s8[8388608]{0:T(1024)(128)(4,1)}), s8[4194304]{0:T(1024)(128)(4,1)S(1)}, s32[]{:S(2)}) async-start(s8[8388608]{0:T(1024)(128)(4,1)} %bitcast.455), calls=%async_computation.3 | async-start | bytes 8388608
  218.0 1.4 copy-start.17
  218.2 17.5 %slice-start.1 = ((s8[8388608]{0:T(1024)(128)(4,1)}), s8[4194304]{0:T(1024)(128)(4,1)S(1)}, s32[]{:S(2)}) async-start(s8[8388608]{0:T(1024)(128)(4,1)} %bitcast.455), calls=%async_computation.4 | async-start | bytes 8388608
  219.0 16.7 %copy-start.13 = (bf16[192,2048]{1,0:T(8,128)(2,1)S(1)}, bf16[192,2048]{1,0:T(8,128)(2,1)}, u32[]{:S(2)}) copy-start(bf16[192,2048]{1,0:T(8,128)(2,1)} %param.16) | copy-start | bytes 2359300
  235.7 2.7 %copy-start.1 = (bf16[2048,256]{1,0:T(8,128)(2,1)S(1)}, bf16[2048,256]{1,0:T(8,128)(2,1)}, u32[]{:S(2)}) copy-start(bf16[2048,256]{1,0:T(8,128)(2,1)} %param.24) | copy-start | bytes 3145732
Sparse Core Ops, SparseCore 0:
  12.6 44.4 all-gather.2
  58.8 40.3 all-gather.4
where the time goes:
time: 250 us; the launch traced here: 246 us
  local copies, waits for them, and re-layouts  63.7 us (25%)
  matrix products  48.7 us (19%)
  blocking collectives  48.6 us (19%)
  other arithmetic  40.8 us (16%)
  waiting for transfers between devices  23 us (9%)
  between operations  14.8 us (6%)
  starting transfers between devices  5.9 us (2%)
    psum x2, blocking collectives, over_axes(): return functools.reduce(lax.psum, axes, shard)  19.2 us
    all_gather x1, waiting for transfers between devices, shards(): piece = lax.all_gather(normed, 'tp', axis=0, tiled=True)  19.1 us
    all_to_all x1, blocking collectives, shards(): lax.all_to_all(attended, 'tp', split_axis=0, concat_axis=1, tiled=True)  16.2 us
    reduce_max x4, other arithmetic, attend_rows(): top = jnp.maximum(jnp.max(s_win, axis=(3, 4)), jnp.max(s_ctx, axis=3))  15.3 us
    dot_general x2, local copies, waits for them, and re-layouts, attend_rows(): jnp.einsum('nir,hrj,ckj->nhcik', row_onehot, offset_bias, col_onehot, pre...  15.2 us
    all_gather x1, blocking collectives, gather_turned(): filled = lax.all_gather(both, axis, axis=0, tiled=True)  13.3 us
    unnamed x93, local copies, waits for them, and re-layouts  12 us
    reduce_sum x4, other arithmetic, attend_rows(): total = jnp.sum(e_win, axis=(3, 4)) + jnp.sum(e_ctx, axis=3)  11 us
  transfers between devices with their start and end apart: 4, of which 2 were waited for; matrix products, arithmetic and copies ran while one was open for 16% of the time, Pallas kernels for 0%

commit v1 on v0

--- a/solution.py
+++ b/solution.py
@@ -158,7 +158,8 @@
     floats = resid.astype(jnp.float32)
     inverse = lax.rsqrt(jnp.mean(floats * floats, axis=-1, keepdims=True) + EPS)
     normed = (floats * inverse * norm_gain * (1.0 + scale) + shift).astype(jnp.bfloat16)
-    piece = lax.all_gather(normed, "tp", axis=0, tiled=True)
+    sent = jnp.stack([normed] * lax.axis_size("tp"))
+    piece = jnp.concatenate(lax.all_to_all(sent, "tp", 0, 0), axis=0)
     queries = head_norm(
         jnp.dot(piece, w_query, preferred_element_type=jnp.float32), query_gain, heads_local
     )

time: 250 us -> 269 us (1.076)
  waiting for transfers between devices: 23 us -> 40.3 us
  matrix products: 48.7 us -> 58.3 us
  other arithmetic: 40.8 us -> 34.6 us
  local copies, waits for them, and re-layouts: 63.7 us -> 58.1 us
  starting transfers between devices: 5.9 us -> 11.1 us
    all_to_all x0 -> x1, waiting for transfers between devices: none -> 23.6 us  [shards(): piece = jnp.concatenate(lax.all_to_all(sent, 'tp', 0, 0), axis=0)]
    all_gather x1 -> x0, waiting for transfers between devices: 19.1 us -> none  [shards(): piece = lax.all_gather(normed, 'tp', axis=0, tiled=True)]
    all_gather x1, waiting for transfers between devices: 0.02 us -> 12.4 us  [side_by_side(): filled, at, done = (lax.all_gather(both, axis, axis=dim, tiled=True), 0, [])]
    dot_general x1, matrix products: 4.67 us -> 16.5 us  [shards(): jnp.dot(piece, w_query, preferred_element_type=jnp.float32)]
    all_to_all x0 -> x1, starting transfers between devices: none -> 4.89 us  [shards(): piece = jnp.concatenate(lax.all_to_all(sent, 'tp', 0, 0), axis=0)]
    slice x4 -> x1, local copies, waits for them, and re-layouts: 4.32 us -> 0.04 us  [shards(): queries[upper:lower]]
    dot_general x0 -> x2, local copies, waits for them, and re-layouts: none -> 4.09 us  [the longest x1 2.3 us: shards(): jnp.dot(piece, w_query, preferred_element_type=jnp.float32)]
    another operation x0 -> x1, local copies, waits for them, and re-layouts: none -> 3.47 us  [shards(): sent = jnp.stack([normed] * lax.axis_size('tp'))]
  transfers between devices with their start and end apart: 4 -> 4, of which waited for: 2 -> 3; matrix products, arithmetic and copies ran while one was open for 16% -> 15% of each run, Pallas kernels for 0% -> 0%
where the time goes in v1:
time: 269 us; the launch traced here: 265 us
  matrix products  58.3 us (22%)
  local copies, waits for them, and re-layouts  58.1 us (22%)
  blocking collectives  48.2 us (18%)
  waiting for transfers between devices  40.3 us (15%)
  other arithmetic  34.6 us (13%)
  between operations  14.6 us (5%)
  starting transfers between devices  11.1 us (4%)
    all_to_all x1, waiting for transfers between devices, shards(): piece = jnp.concatenate(lax.all_to_all(sent, 'tp', 0, 0), axis=0)  23.6 us
    psum x2, blocking collectives, over_axes(): return functools.reduce(lax.psum, axes, shard)  19.2 us
    dot_general x1, matrix products, shards(): jnp.dot(piece, w_query, preferred_element_type=jnp.float32)  16.5 us
    all_to_all x1, blocking collectives, shards(): lax.all_to_all(attended, 'tp', split_axis=0, concat_axis=1, tiled=True)  15.7 us
    dot_general x2, local copies, waits for them, and re-layouts, attend_rows(): jnp.einsum('nir,hrj,ckj->nhcik', row_onehot, offset_bias, col_onehot, pre...  15.3 us
    reduce_max x4, other arithmetic, attend_rows(): top = jnp.maximum(jnp.max(s_win, axis=(3, 4)), jnp.max(s_ctx, axis=3))  15.2 us
    all_gather x1, blocking collectives, gather_turned(): filled = lax.all_gather(both, axis, axis=0, tiled=True)  13.3 us
    all_gather x1, waiting for transfers between devices, side_by_side(): filled, at, done = (lax.all_gather(both, axis, axis=dim, tiled=True), 0, [])  12.4 us
  transfers between devices with their start and end apart: 4, of which 3 were waited for; matrix products, arithmetic and copies ran while one was open for 15% of the time, Pallas kernels for 0%

profile of v1, /device:TPU:24, one launch (start us, length us, event | category | flops | bytes accessed | tf_op | source)
XLA Modules:
  0.0 265.2 jit_solution(11983238386930630671)
XLA Ops:
  6.5 1.1 fusion.125
  7.6 1.0 fusion.123
  8.6 1.0 fusion.121
  9.6 11.7 %all-reduce.1 = (f32[256]{0:T(256)S(1)}, f32[256]{0:T(256)S(1)}, f32[256]{0:T(256)S(1)}) all-reduce(f32[256]{0:T(256)S(1)} %bitcast.459, f32[256]{0:T(256)S(1)} %bitcast.458, f32[256]{0:T(256)S(1)} %bitcast.457), channel_id=1, replica_groups=mesh['sp_0'=4,'sp_1'=4,'tp'=8] {'sp_0'}, use_global_device_ids=true, to_apply=%region_4.5 | all-reduce | flops 768 | bytes 6144 | tf_op jit(solution)/shard_map/psum | solution.py:19
  21.3 7.5 %all-reduce = (f32[256,1]{0,1:T(1,128)S(1)}, f32[256,1]{0,1:T(1,128)S(1)}, f32[256,1]{0,1:T(1,128)S(1)}) all-reduce(f32[256,1]{0,1:T(1,128)S(1)} %bitcast.460, f32[256,1]{0,1:T(1,128)S(1)} %bitcast.461, f32[256,1]{0,1:T(1,128)S(1)} %bitcast.462), channel_id=1, replica_groups=mesh['sp_0'=4,'sp_1'=4,'tp'=8] {'sp_1'}, use_global_device_ids=true, to_apply=%region_5.6 | all-reduce | flops 768 | bytes 6144 | tf_op jit(solution)/shard_map/psum | solution.py:19
  28.8 13.3 %all_gather.6 = f32[2048,3]{0,1:T(4,128)S(1)} all-gather(f32[256,3]{0,1:T(4,128)S(1)} %pad_maximum_fusion.4), channel_id=1, replica_groups=mesh['sp_0'=4,'sp_1'=4,'tp'=8] {'tp'}, dimensions={0}, use_global_device_ids=true | all-gather | bytes 27648 | tf_op jit(solution)/shard_map/all_gather | solution.py:26
  42.1 1.4 fusion.12
  43.5 1.5 fusion.16
  45.0 3.5 %stack.65 = bf16[8,192,2048]{2,1,0:T(8,128)(2,1)} broadcast(bf16[192,2048]{1,0:T(8,128)(2,1)S(1)} %fusion.16), dimensions={1,2} | broadcast | bytes 7077888 | tf_op jit(solution)/shard_map/stack | solution.py:161
  48.5 4.9 %all-to-all-start = ((bf16[8,192,2048]{2,1,0:T(8,128)(2,1)}), bf16[8,192,2048]{2,1,0:T(8,128)(2,1)}, u32[]{:S(2)}, u32[]{:S(2)}) async-start(bf16[8,192,2048]{2,1,0:T(8,128)(2,1)} %stack.65), calls=%async_computation | async-start | bytes 12582912 | tf_op jit(solution)/shard_map/all_to_all | solution.py:162
  54.7 0.6 pad_maximum_fusion.3
  55.4 0.6 convolution_bitcast_fusion.16
  56.1 0.6 gather_fusion.1
  56.8 0.6 gather_fusion.3
  57.3 1.8 copy.578
  59.1 2.3 copy.577
  61.5 5.6 %fusion.108 = f32[64,64,2,16,8]{1,3,4,2,0:T(8,128)} fusion(f32[64,64,2,15,1]{1,3,4,2,0:T(8,128)S(1)} %convolution_bitcast_fusion.16, s32[16,8]{0,1:T(8,128)S(1)} %copy.527), kind=kOutput, calls=%fused_computation.231 | convolution fusion | flops 188745600 | bytes 4686336 | tf_op jit(solution)/shard_map/nir,hrj,ckj->nhcik/dot_general | solution.py:96
  67.1 9.6 %copy.528 = f32[64,64,2,16,8]{0,1,2,3,4:T(8,128)} copy(f32[64,64,2,16,8]{1,3,4,2,0:T(8,128)} %fusion.108) | data formatting | bytes 8388608 | tf_op jit(solution)/shard_map/nir,hrj,ckj->nhcik/dot_general | solution.py:96
  76.9 3.8 %fusion.113 = f32[64,64,2,8,8]{1,4,3,2,0:T(8,128)} fusion(f32[64,64,2,15,1]{1,3,4,2,0:T(8,128)S(1)} %convolution_bitcast_fusion.16, s32[8,8]{1,0:T(8,128)S(1)} %gather_fusion.3), kind=kOutput, calls=%fused_computation.240 | convolution fusion | flops 94372800 | bytes 2588928 | tf_op jit(solution)/shard_map/nir,hrj,ckj->nhcik/dot_general | solution.py:96
  80.7 5.7 %copy.487 = f32[64,64,2,8,8]{0,1,2,3,4:T(8,128)} copy(f32[64,64,2,8,8]{1,4,3,2,0:T(8,128)} %fusion.113) | data formatting | bytes 4194304 | tf_op jit(solution)/shard_map/nir,hrj,ckj->nhcik/dot_general | solution.py:96
  86.4 12.4 %all-gather.2.cloned.1.call-done = bf16[1024,512]{1,0:T(8,128)(2,1)} async-done(((bf16[64,512]{1,0:T(8,128)(2,1)}), bf16[1024,512]{1,0:T(8,128)(2,1)}) %all-gather.2.cloned.1.call-update) | async-done | bytes 1048592 | tf_op jit(solution)/shard_map/all_gather | solution.py:38
  98.8 2.1 fusion.138
  100.9 1.0 reshape.305
  101.9 23.6 %all-to-all-done = bf16[8,192,2048]{2,1,0:T(8,128)(2,1)} async-done(((bf16[8,192,2048]{2,1,0:T(8,128)(2,1)}), bf16[8,192,2048]{2,1,0:T(8,128)(2,1)}, u32[]{:S(2)}, u32[]{:S(2)}) %all-to-all-start) | async-done | bytes 6291488 | tf_op jit(solution)/shard_map/all_to_all | solution.py:162
  125.5 4.6 %multiply_reduce_fusion = (f32[1536,2]{0,1:T(2,128)S(1)}, f32[1536,2,128]{0,2,1:T(8,128)S(1)}) fusion(bf16[1536,2048,1]{1,0,2:T(8,128)(2,1)} %bitcast.15, bf16[2,128,2048]{2,1,0:T(8,128)(2,1)S(1)} %bitcast.443), kind=kOutput, calls=%fused_computation.47 | convolution fusion | flops 1611396096 | bytes 8925184 | tf_op jit(solution)/shard_map/dot_general | solution.py:167
  130.2 4.6 %convolution_convert_fusion = bf16[1536,256]{0,1:T(8,128)(2,1)S(1)} fusion(bf16[1536,2048]{1,0:T(8,128)(2,1)} %bitcast.14, bf16[2048,256]{1,0:T(8,128)(2,1)S(1)} %copy-done), kind=kOutput, calls=%fused_computation.29 | convolution fusion | flops 1611005952 | bytes 8126464 | tf_op jit(solution)/shard_map/dot_general | solution.py:169
  135.0 0.7 copy-done.13
  135.8 1.6 copy.480
  137.4 2.4 concatenate.26
  139.8 7.5 %fusion.137 = (bf16[16,64,1,2,128]{4,3,2,1,0:T(2,128)(2,1)S(1)}, bf16[16,64,1,2,128]{4,3,2,1,0:T(2,128)(2,1)S(1)}, bf16[16,64,1,2,128]{4,3,2,1,0:T(2,128)(2,1)S(...) fusion(bf16[24,64,2,2,128]{4,3,2,1,0:T(2,128)(2,1)S(1)} %concat, ...), kind=kLoop, calls=%fused_computation.283 | loop fusion | bytes 16777216 | tf_op jit(solution)/shard_map/slice | solution.py:210
  147.3 16.5 %multiply_reduce_fusion.1 = (f32[1536,2]{0,1:T(2,128)S(1)}, f32[1536,2,128]{2,0,1:T(8,128)S(1)}) fusion(bf16[1536,2048,1]{1,0,2:T(8,128)(2,1)} %bitcast.15, bf16[2,128,2048]{2,1,0:T(8,128)(2,1)S(1)} %bitcast.442), kind=kOutput, calls=%fused_computation.49 | convolution fusion | flops 1611396096 | bytes 8925184 | tf_op jit(solution)/shard_map/dot_general | solution.py:164
  163.8 0.5 multiply_convert_fusion.1
  164.4 1.3 fusion.58
  168.9 3.2 %copy-done.8 = f32[16,2,64,8,64]{2,4,1,0,3:T(8,128)} copy-done((f32[16,2,64,8,64]{2,4,1,0,3:T(8,128)}, f32[16,2,64,8,64]{2,4,1,0,3:T(8,128)S(1)}, u32[]{:S(2)}) %copy-start.8) | copy-done | bytes 4194328
  172.2 0.9 bitcast_reduce_fusion
  173.1 12.2 %fusion.133 = (f32[16,2,64]{2,1,0:T(2,128)S(1)}, f32[16,2,64,8,64]{2,4,1,0,3:T(8,128)}) fusion(f32[64,64,2,16,8]{0,1,2,3,4:T(8,128)} %copy.528, f32[16,2,64,8,64]{2,4,1,0,3:T(8,128)} %copy-done.8, pred[64,64]{0,1:T(8,128)(4,1)S(1)} %fusion.111), kind=kLoop, calls=%fused_computation.281 | loop fusion | flops 4192256 | bytes 12595200 | tf_op jit(solution)/shard_map/reduce_max | solution.py:118
  185.3 4.6 %fusion.3 = f32[16,2,64]{2,0,1:T(8,128)S(1)} fusion(f32[2,1024,16,64]{1,3,2,0:T(8,128)} %bitcast.418, f32[16,2,64]{2,0,1:T(8,128)S(1)} %copy_maximum_fusion, f32[2]{0:T(128)S(1)} %copy-done.25), kind=kLoop, calls=%fused_computation.14 | loop fusion | flops 8386560 | bytes 8405000 | tf_op jit(solution)/shard_map/reduce_sum | solution.py:121
  189.9 1.6 copy.483
  191.6 1.4 fusion.2
  193.1 1.5 divide_convert_fusion
  194.6 1.0 slice_bitcast_fusion
  195.6 2.4 copy-done.4
  198.0 2.2 fusion.17
  203.1 0.5 copy.550
  203.6 0.9 copy.741
  204.7 4.0 %collective-permute-start = (bf16[4,64,512]{2,1,0:T(8,128)(2,1)S(1)}, bf16[4,64,512]{2,1,0:T(8,128)(2,1)S(1)}, u32[]{:S(2)}, u32[]{:S(2)}) collective-permute-start(bf16[4,64,512]{2,1,0:T(8,128)(2,1)S(1)} %bitcast.452), channel_id=1, source_target_pairs={{0,8},{8,16},{16,24},{24,32},{32,40},{40,48},{48,56},{56,64},{64,7... | collective-permute-start | bytes 786440 | tf_op jit(solution)/shard_map/ppermute | solution.py:53
  208.8 2.1 collective-permute-start.1
  210.9 1.7 gather_fusion
  212.7 0.7 fusion.60
  213.4 1.9 copy-done.5
  215.4 0.5 bitcast_reduce_fusion.1
  216.1 4.3 %collective-permute-done.1 = bf16[4,64,512]{2,1,0:T(8,128)(2,1)S(1)} collective-permute-done((bf16[4,64,512]{2,1,0:T(8,128)(2,1)S(1)}, bf16[4,64,512]{2,1,0:T(8,128)(2,1)S(1)}, u32[]{:S(2)}, u32[]{:S(2)}) %collective-permute-start.1) | collective-permute-done | bytes 262176 | tf_op jit(solution)/shard_map/ppermute | solution.py:55
  220.4 1.7 pad_maximum_fusion
  222.1 3.0 %gather_fusion.2 = bf16[64,64,2,2,128]{4,1,3,2,0:T(8,128)(2,1)} fusion(bf16[32,64,2,2,128]{4,1,3,2,0:T(8,128)(2,1)S(1)} %pad_maximum_fusion, s32[1024]{0:T(1024)S(1)} %pad_clamp_fusion), kind=kCustom, calls=%fused_computation.2 | custom fusion | bytes 8388864 | tf_op jit(solution)/shard_map/jit(_take)/gather | solution.py:194
  225.2 2.6 copy_select_fusion
  230.0 1.6 fusion.135
  231.6 0.6 copy-done.6
  232.2 1.0 fusion.8
  233.2 0.7 fusion.7
  234.0 1.3 fusion.35
  235.6 0.7 divide_convert_fusion.2
  238.6 0.5 fusion.52
  239.5 15.7 %all_to_all.24 = bf16[8,192,256]{2,1,0:T(8,128)(2,1)S(1)} all-to-all(bf16[8,192,256]{2,1,0:T(8,128)(2,1)S(1)} %bitcast.436), channel_id=1, replica_groups=mesh['sp_0'=4,'sp_1'=4,'tp'=8] {'tp'}, dimensions={0} | all-to-all | bytes 1572864 | tf_op jit(solution)/shard_map/all_to_all | solution.py:220
  255.4 2.7 %fusion.10 = bf16[192,2048]{1,0:T(8,128)(2,1)} fusion(bf16[192,2048]{1,0:T(8,128)(2,1)S(1)} %bitcast.444, bf16[2048,2048]{1,0:T(8,128)(2,1)S(1)} %bitcast.464, bf16[192,2048]{1,0:T(8,128)(2,1)S(1)} %copy-done.12, f32[2048]{0:T(1024)S(1)} %bitcast.456), kind=kOutput, calls=%fused_computation.31 | convolution fusion | flops 1612185600 | bytes 10756096 | tf_op jit(solution)/shard_map/dot_general | solution.py:221
  (148 shorter events, 14.0 us)
Async XLA Ops:
  6.5 47.8 %copy-start = (bf16[2048,256]{1,0:T(8,128)(2,1)S(1)}, bf16[2048,256]{1,0:T(8,128)(2,1)}, u32[]{:S(2)}) copy-start(bf16[2048,256]{1,0:T(8,128)(2,1)} %param.25) | copy-start | bytes 3145732
  48.5 5.0 %copy-start.15 = (bf16[64,2048]{1,0:T(8,128)(2,1)S(1)}, bf16[64,2048]{1,0:T(8,128)(2,1)}, u32[]{:S(2)}) copy-start(bf16[64,2048]{1,0:T(8,128)(2,1)} %param.22) | copy-start | bytes 786436
  48.5 5.2 %copy-start.11 = (bf16[2048,256]{1,0:T(8,128)(2,1)S(1)}, bf16[2048,256]{1,0:T(8,128)(2,1)}, u32[]{:S(2)}) copy-start(bf16[2048,256]{1,0:T(8,128)(2,1)} %param.24) | copy-start | bytes 3145732
  48.5 5.2 %copy-start.23 = (f32[2048]{0:T(1024)S(1)}, f32[2048]{0:T(1024)}, u32[]{:S(2)}) copy-start(f32[2048]{0:T(1024)} %param.21) | copy-start | bytes 24580
  48.5 5.7 %copy-start.27 = (f32[128]{0:T(128)S(1)}, f32[128]{0:T(128)}, u32[]{:S(2)}) copy-start(f32[128]{0:T(128)} %param.27) | copy-start | bytes 1540
  48.5 7.0 %copy-start.24 = (f32[2,15,31]{2,0,1:T(2,128)S(1)}, f32[2,15,31]{2,0,1:T(2,128)}, u32[]{:S(2)}) copy-start(f32[2,15,31]{2,0,1:T(2,128)} %param.28) | copy-start | bytes 11164
  48.5 77.0 %all-to-all-start = ((bf16[8,192,2048]{2,1,0:T(8,128)(2,1)}), bf16[8,192,2048]{2,1,0:T(8,128)(2,1)}, u32[]{:S(2)}, u32[]{:S(2)}) async-start(bf16[8,192,2048]{2,1,0:T(8,128)(2,1)} %stack.65), calls=%async_computation | async-start | bytes 12582912 | tf_op jit(solution)/shard_map/all_to_all | solution.py:162
  53.4 2.7 %copy-start.26 = (s32[8]{0:T(128)S(1)}, s32[8]{0:T(128)}, u32[]{:S(2)}) copy-start(s32[8]{0:T(128)} %constant.138) | copy-start | bytes 100
  53.4 45.4 %all-gather.2.cloned.1.call-start = ((), (), s32[]{:S(2)}) async-start(), calls=%async_computation.2 | async-start | bytes 1114112 | tf_op jit(solution)/shard_map/all_gather | solution.py:38
  80.7 44.8 %copy-start.20 = (bf16[256,2048]{1,0:T(8,128)(2,1)S(1)}, bf16[256,2048]{1,0:T(8,128)(2,1)}, u32[]{:S(2)}) copy-start(bf16[256,2048]{1,0:T(8,128)(2,1)} %copy.578) | copy-start | bytes 3145732
  134.8 0.9 copy-start.13
  139.8 7.5 %copy-start.19 = (bf16[256,2048]{1,0:T(8,128)(2,1)S(1)}, bf16[256,2048]{1,0:T(8,128)(2,1)}, u32[]{:S(2)}) copy-start(bf16[256,2048]{1,0:T(8,128)(2,1)} %copy.577) | copy-start | bytes 3145732
  147.2 16.6 %copy-start.28 = (f32[128]{0:T(128)S(1)}, f32[128]{0:T(128)}, u32[]{:S(2)}) copy-start(f32[128]{0:T(128)} %param.26) | copy-start | bytes 1540
  147.2 17.1 %copy-start.10 = (bf16[128,2,8,128]{3,2,1,0:T(8,128)(2,1)S(1)}, bf16[128,2,8,128]{3,2,1,0:T(8,128)(2,1)}, u32[]{:S(2)}) copy-start(bf16[128,2,8,128]{3,2,1,0:T(8,128)(2,1)} %get-tuple-element.58) | copy-start | bytes 1572868
  164.3 1.3 copy-start.9
  165.6 6.5 %copy-start.3 = (f32[2,1024,1024]{1,2,0}, f32[2,1024,1024]{1,2,0:S(1)}, u32[]{:S(2)}) copy-start(f32[2,1024,1024]{1,2,0:S(1)} %fusion.58) | copy-start | bytes 25165828
  167.3 4.9 %copy-start.25 = (f32[2]{0:T(128)S(1)}, f32[2]{0:T(128)}, u32[]{:S(2)}) copy-start(f32[2]{0:T(128)} %param.29) | copy-start | bytes 28
  168.9 3.2 %copy-start.8 = (f32[16,2,64,8,64]{2,4,1,0,3:T(8,128)}, f32[16,2,64,8,64]{2,4,1,0,3:T(8,128)S(1)}, u32[]{:S(2)}) copy-start(f32[16,2,64,8,64]{2,4,1,0,3:T(8,128)S(1)} %fusion.26) | copy-start | bytes 12582916
  185.3 6.2 %copy-start.14 = (bf16[1536,256]{0,1:T(8,128)(2,1)S(1)}, bf16[1536,256]{0,1:T(8,128)(2,1)}, u32[]{:S(2)}) copy-start(bf16[1536,256]{0,1:T(8,128)(2,1)} %copy-done.13) | copy-start | bytes 2359300
  185.3 6.3 %copy-start.2 = (f32[16,2,64,8,64]{2,4,1,0,3:T(8,128)S(1)}, f32[16,2,64,8,64]{2,4,1,0,3:T(8,128)}, u32[]{:S(2)}) copy-start(f32[16,2,64,8,64]{2,4,1,0,3:T(8,128)} %get-tuple-element.12) | copy-start | bytes 12582916
  193.1 2.6 copy-start.21
  194.6 3.4 %copy-start.4 = (f32[2,1024,1024]{1,2,0:S(1)}, f32[2,1024,1024]{1,2,0}, u32[]{:S(2)}) copy-start(f32[2,1024,1024]{1,2,0} %copy-done.3) | copy-start | bytes 25165828
  198.0 2.2 copy-start.18
  198.0 2.5 copy-start.17
  204.7 11.3 %collective-permute-start = (bf16[4,64,512]{2,1,0:T(8,128)(2,1)S(1)}, bf16[4,64,512]{2,1,0:T(8,128)(2,1)S(1)}, u32[]{:S(2)}, u32[]{:S(2)}) collective-permute-start(bf16[4,64,512]{2,1,0:T(8,128)(2,1)S(1)} %bitcast.452), channel_id=1, source_target_pairs={{0,8},{8,16},{16,24},{24,32},{32,40},{40,48},{48,56},{56,64},{64,7... | collective-permute-start | bytes 786440 | tf_op jit(solution)/shard_map/ppermute | solution.py:53
  208.8 11.5 %collective-permute-start.1 = (bf16[4,64,512]{2,1,0:T(8,128)(2,1)S(1)}, bf16[4,64,512]{2,1,0:T(8,128)(2,1)S(1)}, u32[]{:S(2)}, u32[]{:S(2)}) collective-permute-start(bf16[4,64,512]{2,1,0:T(8,128)(2,1)S(1)} %bitcast.451), channel_id=1, source_target_pairs={{8,0},{16,8},{24,16},{32,24},{40,32},{48,40},{56,48},{64,56},{72,6... | collective-permute-start | bytes 786440 | tf_op jit(solution)/shard_map/ppermute | solution.py:55
  213.4 2.0 copy-start.5
  227.8 2.2 copy-start.7
  230.0 2.2 copy-start.6
  232.2 1.8 copy-start.22
  236.4 18.9 %slice-start = ((s8[8388608]{0:T(1024)(128)(4,1)}), s8[4194304]{0:T(1024)(128)(4,1)S(1)}, s32[]{:S(2)}) async-start(s8[8388608]{0:T(1024)(128)(4,1)} %bitcast.463), calls=%async_computation.3 | async-start | bytes 8388608
  238.0 1.4 copy-start.16
  238.3 17.0 %slice-start.1 = ((s8[8388608]{0:T(1024)(128)(4,1)}), s8[4194304]{0:T(1024)(128)(4,1)S(1)}, s32[]{:S(2)}) async-start(s8[8388608]{0:T(1024)(128)(4,1)} %bitcast.463), calls=%async_computation.4 | async-start | bytes 8388608
  239.1 16.3 %copy-start.12 = (bf16[192,2048]{1,0:T(8,128)(2,1)S(1)}, bf16[192,2048]{1,0:T(8,128)(2,1)}, u32[]{:S(2)}) copy-start(bf16[192,2048]{1,0:T(8,128)(2,1)} %param.16) | copy-start | bytes 2359300
  255.3 2.7 %copy-start.1 = (bf16[2048,256]{1,0:T(8,128)(2,1)S(1)}, bf16[2048,256]{1,0:T(8,128)(2,1)}, u32[]{:S(2)}) copy-start(bf16[2048,256]{1,0:T(8,128)(2,1)} %param.25) | copy-start | bytes 3145732
Sparse Core Ops, SparseCore 0:
  56.3 42.3 all-gather.1
